TPU v7x, 256 devices: a whole 4x4x8 slice. The times are simulated.
256 devices in a mesh: ra: 32 (over z, y), cb: 8 (over x, core).
Axes of the slice: x: 4, y: 4, z: 8, core: 2. Of those that a mesh axis runs over, the one named last changes fastest.
Arguments:
- tokens: bfloat16 [2048, 16384], P('ra'), may hold values from -16 to 16
- norm_gain: float32 [2, 2048], replicated, may hold values from 0.1 to 1.9
- up_weight: float32 [2, 2048, 6144], P(None, 'ra', 'cb'), may hold values from -0.125 to 0.125
- gate_weight: float32 [2, 2048, 6144], P(None, 'ra', 'cb'), may hold values from -0.125 to 0.125
- up_scale: float32 [2, 6144], P(None, 'cb'), may hold values from 0.5 to 2
- gate_scale: float32 [2, 6144], P(None, 'cb'), may hold values from 0.5 to 2
- up_taps: float32 [2, 3, 6144], P(None, None, 'cb'), may hold values from -3 to 3
- gate_taps: float32 [2, 3, 6144], P(None, None, 'cb'), may hold values from -3 to 3
- down_weight: float32 [2, 2048, 6144], P(None, 'ra', 'cb'), may hold values from -0.078125 to 0.078125
- down_scale: float32 [2, 2048], replicated, may hold values from 0.5 to 2
Outputs:
- mixed: bfloat16 [2048, 16384], P('ra')
All inputs are finite; a program needn't handle non-finite values.
Results may differ from a plain program's by a relative error of at most 0.024.
Values may be sent and summed in bfloat16 or wider, within the bound.
No kernel may reach another device: no remote copies, remote signals or barrier semaphores. Data moves between devices by JAX's collectives and lax.ppermute only.
A program may use at most 64 MiB of HBM per device.

v0:
```python
import jax
import jax.numpy as jnp
from jax import lax
from jax.sharding import Mesh
from jax.sharding import PartitionSpec as P

RA = ("ra_0", "ra_1")
EPS = 1e-06
RESIDUAL = 0.5


def shifted(value, axis, steps):
    count = lax.axis_size(axis)
    initial, last = (max(0, -steps), min(count, count - steps))
    return lax.ppermute(value, axis, [(source, source + steps) for source in range(initial, last)])


def sent_together(arrays, axis, dim, along):
    ends, at = ([], 0)
    for a in arrays[:-1]:
        at += a.shape[along]
        ends.append(at)
    both = jnp.concatenate(arrays, axis=along)
    return tuple(jnp.split(lax.all_gather(both, axis, axis=dim, tiled=True), ends, axis=along))


def gather_axes(value, axes, dim):
    whole = value
    for number in range(len(axes) - 1, -1, -1):
        whole = lax.all_gather(whole, axes[number], axis=dim, tiled=True)
    return whole


def padded_to(lines, length):
    spare = -len(lines) % length
    return jnp.pad(lines, [(0, spare)] + [(0, 0)] * (lines.ndim - 1))


def total_of(value, axis):
    lines = value.reshape(-1, *value.shape[1:][-1:])
    own = lax.psum_scatter(
        padded_to(lines, lax.axis_size(axis)), axis, scatter_dimension=0, tiled=True
    )
    whole = lax.all_gather(own, axis).reshape(-1, *lines.shape[1:])
    return lax.slice_in_dim(whole, 0, len(lines)).reshape(value.shape)


def valid_taps(values, taps):
    width = taps.shape[0]
    length = values.shape[0] - width + 1
    total = taps[0][None, :] * values[0:length]
    for k in range(1, width):
        total = total + taps[k][None, :] * values[k : k + length]
    return total


def per_device(
    tokens,
    norm_gain,
    up_weight,
    gate_weight,
    up_scale,
    gate_scale,
    up_taps,
    gate_taps,
    down_weight,
    down_scale,
):
    state = lax.all_to_all(tokens, RA, split_axis=1, concat_axis=0, tiled=True).T
    edge = up_taps.shape[1] - 1
    for layer in range(up_weight.shape[0]):
        before = shifted(state[state.shape[0] - edge :], RA, 1)
        rows = jnp.concatenate([before, state], axis=0)
        rows_f = rows.astype(jnp.float32)
        inverse = lax.rsqrt(jnp.mean(rows_f * rows_f, axis=1, keepdims=True) + EPS)
        scaled = (rows_f * norm_gain[layer][None, :]).astype(jnp.bfloat16)
        pieces = sent_together(
            (up_weight[layer].astype(jnp.bfloat16), gate_weight[layer].astype(jnp.bfloat16)),
            RA,
            0,
            1,
        )
        up_raw = jnp.dot(scaled, pieces[0], preferred_element_type=jnp.float32)
        gate_raw = jnp.dot(scaled, pieces[1], preferred_element_type=jnp.float32)
        up_pre = up_raw * inverse * up_scale[layer][None, :]
        gate_pre = gate_raw * inverse * gate_scale[layer][None, :]
        conv_up = valid_taps(up_pre, up_taps[layer])
        conv_gate = valid_taps(gate_pre, gate_taps[layer])
        hidden = (jax.nn.silu(conv_gate) * conv_up).astype(jnp.bfloat16)
        down_part = lax.dot_general(
            hidden,
            gather_axes(down_weight[layer].astype(jnp.bfloat16), RA, 0),
            (((1,), (1,)), ((), ())),
            preferred_element_type=jnp.float32,
        )
        down = total_of(down_part.astype(jnp.bfloat16), "cb").astype(jnp.float32)
        state = (down * down_scale[layer][None, :] + RESIDUAL * state.astype(jnp.float32)).astype(
            jnp.bfloat16
        )
    return lax.all_to_all(state.T, RA, split_axis=0, concat_axis=1, tiled=True)


def solution(mesh):
    torus = Mesh(mesh.devices.reshape(8, 4, mesh.shape["cb"]), ("ra_0", "ra_1", "cb"))
    placed = (
        P(RA, None),
        P(),
        P(None, RA, "cb"),
        P(None, RA, "cb"),
        P(None, "cb"),
        P(None, "cb"),
        P(None, None, "cb"),
        P(None, None, "cb"),
        P(None, RA, "cb"),
        P(),
    )
    return jax.shard_map(
        per_device, mesh=torus, in_specs=placed, out_specs=P(RA, None), check_vma=False
    )
```

profile of v0, /device:TPU:8, one launch (start us, length us, event | category | flops | bytes accessed | tf_op | source)
XLA Modules:
  0.0 512.2 jit_solution(13660260227973896724)
XLA Ops:
  11.1 11.8 %all-to-all-start = ((bf16[64,32,512]{2,0,1:T(8,128)(2,1)}), bf16[64,32,512]{2,0,1:T(8,128)(2,1)S(1)}, u32[]{:S(2)}, u32[]{:S(2)}) async-start(bf16[64,32,512]{2,0,1:T(8,128)(2,1)} %bitcast.42), calls=%async_computation | async-start | bytes 4194304 | tf_op jit(solution)/shard_map/all_to_all | solution.py:69
  23.1 19.1 %all-gather = bf16[1,256,768]{2,1,0:T(8,128)(2,1)} all-gather(bf16[1,64,768]{2,1,0:T(8,128)(2,1)S(1)} %get-tuple-element.26), channel_id=2, replica_groups=mesh['ra_0'=8,'ra_1'=4,'cb'=8] {'ra_1'}, dimensions={1}, use_global_device_ids=true | all-gather | bytes 491520 | tf_op jit(solution)/shard_map/all_gather | solution.py:30
  42.5 37.1 %all-to-all-done = bf16[64,32,512]{2,0,1:T(8,128)(2,1)S(1)} async-done(((bf16[64,32,512]{2,0,1:T(8,128)(2,1)}), bf16[64,32,512]{2,0,1:T(8,128)(2,1)S(1)}, u32[]{:S(2)}, u32[]{:S(2)}) %all-to-all-start) | async-done | bytes 2097184 | tf_op jit(solution)/shard_map/all_to_all | solution.py:69
  80.9 3.0 copy.20
  83.9 3.9 collective-permute-start
  90.6 20.9 %all-gather.13.cloned.1.call-done = bf16[2048,1536]{1,0:T(8,128)(2,1)} async-done(((bf16[64,1536]{1,0:T(8,128)(2,1)}), bf16[2048,1536]{1,0:T(8,128)(2,1)}) %all-gather.13.cloned.1.call-update) | async-done | bytes 6291472 | tf_op jit(solution)/shard_map/all_gather | solution.py:24
  111.5 5.2 %multiply_multiply_fusion.3 = f32[514,768]{1,0:T(8,128)} fusion(bf16[2048,1536]{1,0:T(8,128)(2,1)} %all-gather.13.cloned.1.call-done, f32[2048]{0:T(1024)S(1)} %bitcast.50, f32[768]{0:T(1024)S(1)} %get-tuple-element.18, f32[514]{0:T(1024)S(1)} %add_rsqrt_fusion.1, bf16[512,2048]{1,0:T(8,128)(2,1)S(1)} %bitcast.39, bf16[2,2048]{1,0:T(2,128)(2,1)S(1)} %collective-permute-done), kind=kOutput, calls=%fused_computation.35 | convolution fusion | flops 1624009728 | bytes 6843400 | tf_op jit(solution)/shard_map/dot_general | solution.py:84
  116.7 3.1 multiply_multiply_fusion.2
  119.8 36.8 %all-gather.17.cloned.1.call-done = bf16[1,2048,768]{2,1,0:T(8,128)(2,1)} async-done(((bf16[1,256,768]{2,1,0:T(8,128)(2,1)}), bf16[1,2048,768]{2,1,0:T(8,128)(2,1)}) %all-gather.17.cloned.1.call-update) | async-done | bytes 3145744 | tf_op jit(solution)/shard_map/all_gather | solution.py:30
  156.5 8.9 %fusion.20 = bf16[512,2048]{1,0:T(8,128)(2,1)} fusion(bf16[1,2048,768]{2,1,0:T(8,128)(2,1)} %all-gather.17.cloned.1.call-done, f32[514,768]{1,0:T(8,128)} %multiply_multiply_fusion.2, f32[514,768]{1,0:T(8,128)} %multiply_multiply_fusion.3, f32[768]{0:T(1024)S(1)} %get-tuple-element.12, f32[768]{0:T(1024)S(1)} %get-tuple-element.13, ...), kind=kOutput, calls=%fused_computation.26 | convolution fusion | flops 1617952768 | bytes 14698496 | tf_op jit(solution)/shard_map/dot_general | solution.py:90
  165.5 35.1 %reduce-scatter.3.cloned.1.call-done = bf16[64,2048]{1,0:T(8,128)(2,1)} async-done(((bf16[512,2048]{1,0:T(8,128)(2,1)}), bf16[64,2048]{1,0:T(8,128)(2,1)}) %reduce-scatter.3.cloned.1.call-update) | async-done | bytes 262160 | tf_op jit(solution)/shard_map/reduce_scatter | solution.py:41
  201.4 13.3 %all-gather.3 = bf16[1,256,768]{2,1,0:T(8,128)(2,1)} all-gather(bf16[1,64,768]{2,1,0:T(8,128)(2,1)S(1)} %get-tuple-element.25), channel_id=5, replica_groups=mesh['ra_0'=8,'ra_1'=4,'cb'=8] {'ra_1'}, dimensions={1}, use_global_device_ids=true | all-gather | bytes 491520 | tf_op jit(solution)/shard_map/all_gather | solution.py:30
  214.8 14.2 %all-gather.19.cloned.1.call-done = bf16[512,2048]{1,0:T(8,128)(2,1)} async-done(((bf16[64,2048]{1,0:T(8,128)(2,1)}), bf16[512,2048]{1,0:T(8,128)(2,1)}) %all-gather.19.cloned.1.call-update) | async-done | bytes 2097168 | tf_op jit(solution)/shard_map/all_gather | solution.py:44
  231.5 3.6 collective-permute-start.1
  237.9 80.9 %all-gather.15.cloned.1.call-done = bf16[2048,1536]{1,0:T(8,128)(2,1)} async-done(((bf16[64,1536]{1,0:T(8,128)(2,1)}), bf16[2048,1536]{1,0:T(8,128)(2,1)}) %all-gather.15.cloned.1.call-update) | async-done | bytes 6291472 | tf_op jit(solution)/shard_map/all_gather | solution.py:24
  318.8 5.8 %multiply_multiply_fusion.1 = f32[514,768]{1,0:T(8,128)} fusion(bf16[2048,1536]{1,0:T(8,128)(2,1)} %all-gather.15.cloned.1.call-done, f32[2048]{0:T(1024)S(1)} %bitcast.48, f32[768]{0:T(1024)S(1)} %get-tuple-element.17, f32[514]{0:T(1024)S(1)} %add_rsqrt_fusion, bf16[512,2048]{1,0:T(8,128)(2,1)} %copy-done, bf16[2,2048]{1,0:T(2,128)(2,1)S(1)} %collective-permute-done.1), kind=kOutput, calls=%fused_computation.33 | convolution fusion | flops 1624009728 | bytes 6843400 | tf_op jit(solution)/shard_map/dot_general | solution.py:84
  324.6 3.1 multiply_multiply_fusion
  327.7 36.0 %all-gather.21.cloned.1.call-done = bf16[1,2048,768]{2,1,0:T(8,128)(2,1)} async-done(((bf16[1,256,768]{2,1,0:T(8,128)(2,1)}), bf16[1,2048,768]{2,1,0:T(8,128)(2,1)}) %all-gather.21.cloned.1.call-update) | async-done | bytes 3145744 | tf_op jit(solution)/shard_map/all_gather | solution.py:30
  363.7 8.9 %fusion.23 = bf16[512,2048]{1,0:T(8,128)(2,1)} fusion(bf16[1,2048,768]{2,1,0:T(8,128)(2,1)} %all-gather.21.cloned.1.call-done, f32[514,768]{1,0:T(8,128)} %multiply_multiply_fusion, f32[514,768]{1,0:T(8,128)} %multiply_multiply_fusion.1, f32[768]{0:T(1024)S(1)} %get-tuple-element.15, f32[768]{0:T(1024)S(1)} %get-tuple-element.16, ...), kind=kOutput, calls=%fused_computation.27 | convolution fusion | flops 1617952768 | bytes 14698496 | tf_op jit(solution)/shard_map/dot_general | solution.py:90
  372.6 35.1 %reduce-scatter.5.cloned.1.call-done = bf16[64,2048]{1,0:T(8,128)(2,1)} async-done(((bf16[512,2048]{1,0:T(8,128)(2,1)}), bf16[64,2048]{1,0:T(8,128)(2,1)}) %reduce-scatter.5.cloned.1.call-update) | async-done | bytes 262160 | tf_op jit(solution)/shard_map/reduce_scatter | solution.py:41
  407.7 28.6 %all-gather.23.cloned.1.call-done = bf16[512,2048]{1,0:T(8,128)(2,1)} async-done(((bf16[64,2048]{1,0:T(8,128)(2,1)}), bf16[512,2048]{1,0:T(8,128)(2,1)}) %all-gather.23.cloned.1.call-update) | async-done | bytes 2097168 | tf_op jit(solution)/shard_map/all_gather | solution.py:44
  436.3 3.8 fusion.26
  440.1 2.9 copy.21
  443.0 60.9 %all_to_all.38 = bf16[32,64,512]{2,1,0:T(8,128)(2,1)S(1)} all-to-all(bf16[32,64,512]{2,1,0:T(8,128)(2,1)S(1)} %bitcast.43), channel_id=1, replica_groups=mesh['ra_0'=8,'ra_1'=4,'cb'=8] {'ra_0','ra_1'}, dimensions={0} | all-to-all | bytes 4194304 | tf_op jit(solution)/shard_map/all_to_all | solution.py:100
  (65 shorter events, 16.7 us)
Async XLA Ops:
  6.5 3.0 copy-start.3
  6.5 105.0 %all-gather.13.cloned.1.call-start = ((), (), s32[]{:S(2)}) async-start(), calls=%async_computation.4 | async-start | bytes 6488064 | tf_op jit(solution)/shard_map/all_gather | solution.py:24
  11.1 11.9 %copy-start.4 = (f32[2,64,768]{2,1,0:T(8,128)S(1)}, f32[2,64,768]{2,1,0:T(8,128)}, u32[]{:S(2)}) copy-start(f32[2,64,768]{2,1,0:T(8,128)} %param.18) | copy-start | bytes 1179652
  11.1 31.2 %copy-start.9 = (f32[2,768]{1,0:T(2,128)S(1)}, f32[2,768]{1,0:T(2,128)}, u32[]{:S(2)}) copy-start(f32[2,768]{1,0:T(2,128)} %param.15) | copy-start | bytes 18436
  11.1 31.2 %copy-start.5 = (f32[2,3,768]{2,0,1:T(2,128)S(1)}, f32[2,3,768]{2,0,1:T(2,128)}, u32[]{:S(2)}) copy-start(f32[2,3,768]{2,0,1:T(2,128)} %param.16) | copy-start | bytes 55300
  11.1 31.2 %copy-start.6 = (f32[2,3,768]{2,0,1:T(2,128)S(1)}, f32[2,3,768]{2,0,1:T(2,128)}, u32[]{:S(2)}) copy-start(f32[2,3,768]{2,0,1:T(2,128)} %param.17) | copy-start | bytes 55300
  11.1 31.4 %copy-start.7 = (f32[2,2048]{1,0:T(2,128)S(1)}, f32[2,2048]{1,0:T(2,128)}, u32[]{:S(2)}) copy-start(f32[2,2048]{1,0:T(2,128)} %param.11) | copy-start | bytes 49156
  11.1 68.5 %all-to-all-start = ((bf16[64,32,512]{2,0,1:T(8,128)(2,1)}), bf16[64,32,512]{2,0,1:T(8,128)(2,1)S(1)}, u32[]{:S(2)}, u32[]{:S(2)}) async-start(bf16[64,32,512]{2,0,1:T(8,128)(2,1)} %bitcast.42), calls=%async_computation | async-start | bytes 4194304 | tf_op jit(solution)/shard_map/all_to_all | solution.py:69
  23.0 133.5 %all-gather.17.cloned.1.call-start = ((), (), s32[]{:S(2)}) async-start(), calls=%async_computation.8 | async-start | bytes 3538944 | tf_op jit(solution)/shard_map/all_gather | solution.py:30
  42.3 158.3 %reduce-scatter.3.cloned.1.call-start = ((), (), s32[]{:S(2)}) async-start(), calls=%async_computation.5 | async-start | bytes 2359296 | tf_op jit(solution)/shard_map/reduce_scatter | solution.py:41
  79.6 1.3 copy-start.2
  80.9 6.9 %copy-start.10 = (f32[2,768]{1,0:T(2,128)S(1)}, f32[2,768]{1,0:T(2,128)}, u32[]{:S(2)}) copy-start(f32[2,768]{1,0:T(2,128)} %param.14) | copy-start | bytes 18436
  83.9 5.8 %collective-permute-start = (bf16[2,2048]{1,0:T(2,128)(2,1)S(1)}, bf16[2,2048]{1,0:T(2,128)(2,1)S(1)}, u32[]{:S(2)}, u32[]{:S(2)}) collective-permute-start(bf16[2,2048]{1,0:T(2,128)(2,1)S(1)} %slice.194), channel_id=1, source_target_pairs={{0,8},{8,16},{16,24},{24,32},{32,40},{40,48},{48,56},{56,64},{64,7... | collective-permute-start | bytes 24584 | tf_op jit(solution)/shard_map/ppermute | solution.py:15
  111.5 5.2 %copy-start.11 = (bf16[2048,1536]{1,0:T(8,128)(2,1)S(1)}, bf16[2048,1536]{1,0:T(8,128)(2,1)}, u32[]{:S(2)}) copy-start(bf16[2048,1536]{1,0:T(8,128)(2,1)} %all-gather.13.cloned.1.call-done) | copy-start | bytes 18874372
  165.4 49.4 %copy-start.8 = (f32[2,2048]{1,0:T(2,128)S(1)}, f32[2,2048]{1,0:T(2,128)}, u32[]{:S(2)}) copy-start(f32[2,2048]{1,0:T(2,128)} %param.19) | copy-start | bytes 49156
  165.5 63.6 %all-gather.19.cloned.1.call-start = ((), (), s32[]{:S(2)}) async-start(), calls=%async_computation.9 | async-start | bytes 2359296 | tf_op jit(solution)/shard_map/all_gather | solution.py:44
  200.6 118.2 %all-gather.15.cloned.1.call-start = ((), (), s32[]{:S(2)}) async-start(), calls=%async_computation.6 | async-start | bytes 6488064 | tf_op jit(solution)/shard_map/all_gather | solution.py:24
  201.4 162.3 %all-gather.21.cloned.1.call-start = ((), (), s32[]{:S(2)}) async-start(), calls=%async_computation.10 | async-start | bytes 3538944 | tf_op jit(solution)/shard_map/all_gather | solution.py:30
  214.7 193.0 %reduce-scatter.5.cloned.1.call-start = ((), (), s32[]{:S(2)}) async-start(), calls=%async_computation.7 | async-start | bytes 2359296 | tf_op jit(solution)/shard_map/reduce_scatter | solution.py:41
  231.5 5.6 %copy-start = (bf16[512,2048]{1,0:T(8,128)(2,1)}, bf16[512,2048]{1,0:T(8,128)(2,1)S(1)}, u32[]{:S(2)}) copy-start(bf16[512,2048]{1,0:T(8,128)(2,1)S(1)} %fusion.7) | copy-start | bytes 6291460
  231.5 5.5 %collective-permute-start.1 = (bf16[2,2048]{1,0:T(2,128)(2,1)S(1)}, bf16[2,2048]{1,0:T(2,128)(2,1)S(1)}, u32[]{:S(2)}, u32[]{:S(2)}) collective-permute-start(bf16[2,2048]{1,0:T(2,128)(2,1)S(1)} %slice.204), channel_id=1, source_target_pairs={{0,8},{8,16},{16,24},{24,32},{32,40},{40,48},{48,56},{56,64},{64,7... | collective-permute-start | bytes 24584 | tf_op jit(solution)/shard_map/ppermute | solution.py:15
  318.8 5.8 %copy-start.1 = (bf16[512,2048]{1,0:T(8,128)(2,1)S(1)}, bf16[512,2048]{1,0:T(8,128)(2,1)}, u32[]{:S(2)}) copy-start(bf16[512,2048]{1,0:T(8,128)(2,1)} %copy-done) | copy-start | bytes 6291460
  318.8 5.8 %copy-start.12 = (bf16[2048,1536]{1,0:T(8,128)(2,1)S(1)}, bf16[2048,1536]{1,0:T(8,128)(2,1)}, u32[]{:S(2)}) copy-start(bf16[2048,1536]{1,0:T(8,128)(2,1)} %all-gather.15.cloned.1.call-done) | copy-start | bytes 18874372
  372.6 63.7 %all-gather.23.cloned.1.call-start = ((), (), s32[]{:S(2)}) async-start(), calls=%async_computation.11 | async-start | bytes 2359296 | tf_op jit(solution)/shard_map/all_gather | solution.py:44
Sparse Core Ops, SparseCore 0:
  9.9 101.5 all-gather.12
  113.3 43.1 all-gather.16
  165.6 34.9 reduce-scatter.2
  202.3 26.6 all-gather.18
  231.4 87.3 all-gather.14
  320.5 43.1 all-gather.20
  372.7 34.9 reduce-scatter.4
  409.6 26.6 all-gather.22
where the time goes:
time: 513 us; the launch traced here: 512 us
  waiting for transfers between devices  328 us (64%)
  blocking collectives  93.3 us (18%)
  matrix products  34.9 us (7%)
  starting transfers between devices  19.6 us (4%)
  between operations  13.7 us (3%)
  other arithmetic  11.6 us (2%)
  local copies, waits for them, and re-layouts  10.6 us (2%)
    all_gather x2, waiting for transfers between devices, sent_together(): lax.all_gather(both, axis, axis=dim, tiled=True)  102 us
    all_gather x2, waiting for transfers between devices, gather_axes(): whole = lax.all_gather(whole, axes[number], axis=dim, tiled=True)  72.7 us
    reduce_scatter x2, waiting for transfers between devices, total_of(): lax.psum_scatter(padded_to(lines, lax.axis_size(axis)), axis, scatter_dim...  70.1 us
    all_to_all x1, blocking collectives, per_device(): return lax.all_to_all(state.T, RA, split_axis=0, concat_axis=1, tiled=True)  60.9 us
    all_gather x2, waiting for transfers between devices, total_of(): whole = lax.all_gather(own, axis).reshape(-1, *lines.shape[1:])  42.7 us
    all_to_all x1, waiting for transfers between devices, per_device(): lax.all_to_all(tokens, RA, split_axis=1, concat_axis=0, tiled=True)  37.1 us
    all_gather x2, blocking collectives, gather_axes(): whole = lax.all_gather(whole, axes[number], axis=dim, tiled=True)  32.4 us
    dot_general x2, matrix products, per_device(): lax.dot_general(hidden, gather_axes(down_weight[layer].astype(jnp.bfloat1...  17.8 us
  transfers between devices with their start and end apart: 11, of which 11 were waited for; matrix products, arithmetic and copies ran while one was open for 5% of the time, Pallas kernels for 0%

commit v1 on v0

--- a/solution.py
+++ b/solution.py
@@ -7,6 +7,13 @@
 RA = ("ra_0", "ra_1")
 EPS = 1e-06
 RESIDUAL = 0.5
+
+
+def exchange_blocks(block, axis, split, join):
+    count = lax.axis_size(axis)
+    blocks = jnp.stack(jnp.split(block, count, axis=split), axis=0)
+    blocks = lax.all_to_all(blocks, axis, split_axis=0, concat_axis=0)
+    return jnp.concatenate(blocks, axis=join)
 
 
 def shifted(value, axis, steps):
@@ -66,7 +73,7 @@
     down_weight,
     down_scale,
 ):
-    state = lax.all_to_all(tokens, RA, split_axis=1, concat_axis=0, tiled=True).T
+    state = exchange_blocks(tokens, RA, 1, 0).T
     edge = up_taps.shape[1] - 1
     for layer in range(up_weight.shape[0]):
         before = shifted(state[state.shape[0] - edge :], RA, 1)

time: 513 us -> 524 us (1.021)
  local copies, waits for them, and re-layouts: 10.6 us -> 29.2 us
    unnamed x26 -> x57, local copies, waits for them, and re-layouts: 1.37 us -> 21 us
    all_gather x2, waiting for transfers between devices: 102 us -> 87.2 us  [sent_together(): lax.all_gather(both, axis, axis=dim, tiled=True)]
    all_to_all x1, waiting for transfers between devices: 37.1 us -> 48.2 us  [exchange_blocks(): blocks = lax.all_to_all(blocks, axis, split_axis=0, concat_axis=0)]
  transfers between devices with their start and end apart: 11 -> 11, of which waited for: 11 -> 11; matrix products, arithmetic and copies ran while one was open for 5% -> 9% of each run, Pallas kernels for 0% -> 0%
where the time goes in v1:
time: 524 us; the launch traced here: 523 us
  waiting for transfers between devices  325 us (62%)
  blocking collectives  88.7 us (17%)
  matrix products  34.9 us (7%)
  local copies, waits for them, and re-layouts  29.2 us (6%)
  starting transfers between devices  19.6 us (4%)
  between operations  13.7 us (3%)
  other arithmetic  11.6 us (2%)
    all_gather x2, waiting for transfers between devices, sent_together(): lax.all_gather(both, axis, axis=dim, tiled=True)  87.2 us
    all_gather x2, waiting for transfers between devices, gather_axes(): whole = lax.all_gather(whole, axes[number], axis=dim, tiled=True)  73.4 us
    reduce_scatter x2, waiting for transfers between devices, total_of(): lax.psum_scatter(padded_to(lines, lax.axis_size(axis)), axis, scatter_dim...  70.1 us
    all_to_all x1, blocking collectives, per_device(): return lax.all_to_all(state.T, RA, split_axis=0, concat_axis=1, tiled=True)  60.9 us
    all_to_all x1, waiting for transfers between devices, exchange_blocks(): blocks = lax.all_to_all(blocks, axis, split_axis=0, concat_axis=0)  48.2 us
    all_gather x2, waiting for transfers between devices, total_of(): whole = lax.all_gather(own, axis).reshape(-1, *lines.shape[1:])  42.7 us
    all_gather x2, blocking collectives, gather_axes(): whole = lax.all_gather(whole, axes[number], axis=dim, tiled=True)  27.9 us
    unnamed x57, local copies, waits for them, and re-layouts  21 us
  transfers between devices with their start and end apart: 11, of which 11 were waited for; matrix products, arithmetic and copies ran while one was open for 9% of the time, Pallas kernels for 0%

profile of v1, /device:TPU:8, one launch (start us, length us, event | category | flops | bytes accessed | tf_op | source)
XLA Modules:
  0.0 523.1 jit_solution(11889408912213434894)
XLA Ops:
  29.8 11.8 %all-to-all-start = ((bf16[32,64,512]{2,1,0:T(8,128)(2,1)}), bf16[32,64,512]{2,1,0:T(8,128)(2,1)S(1)}, u32[]{:S(2)}, u32[]{:S(2)}) async-start(bf16[32,64,512]{2,1,0:T(8,128)(2,1)} %constant_dynamic-update-slice_fusion), calls=%async_computation | async-start | bytes 4194304 | tf_op jit(solution)/shard_map/all_to_all | solution.py:15
  41.8 14.6 %all-gather = bf16[1,256,768]{2,1,0:T(8,128)(2,1)} all-gather(bf16[1,64,768]{2,1,0:T(8,128)(2,1)S(1)} %get-tuple-element.26), channel_id=2, replica_groups=mesh['ra_0'=8,'ra_1'=4,'cb'=8] {'ra_1'}, dimensions={1}, use_global_device_ids=true | all-gather | bytes 491520 | tf_op jit(solution)/shard_map/all_gather | solution.py:37
  56.6 48.2 %all-to-all-done = bf16[32,64,512]{2,1,0:T(8,128)(2,1)S(1)} async-done(((bf16[32,64,512]{2,1,0:T(8,128)(2,1)}), bf16[32,64,512]{2,1,0:T(8,128)(2,1)S(1)}, u32[]{:S(2)}, u32[]{:S(2)}) %all-to-all-start) | async-done | bytes 2097184 | tf_op jit(solution)/shard_map/all_to_all | solution.py:15
  106.1 2.9 copy.15
  109.1 3.9 collective-permute-start
  115.5 6.3 %all-gather.13.cloned.1.call-done = bf16[2048,1536]{1,0:T(8,128)(2,1)} async-done(((bf16[64,1536]{1,0:T(8,128)(2,1)}), bf16[2048,1536]{1,0:T(8,128)(2,1)}) %all-gather.13.cloned.1.call-update) | async-done | bytes 6291472 | tf_op jit(solution)/shard_map/all_gather | solution.py:31
  121.7 5.2 multiply_multiply_fusion.3
  126.9 3.1 multiply_multiply_fusion.2
  130.0 37.4 %all-gather.17.cloned.1.call-done = bf16[1,2048,768]{2,1,0:T(8,128)(2,1)} async-done(((bf16[1,256,768]{2,1,0:T(8,128)(2,1)}), bf16[1,2048,768]{2,1,0:T(8,128)(2,1)}) %all-gather.17.cloned.1.call-update) | async-done | bytes 3145744 | tf_op jit(solution)/shard_map/all_gather | solution.py:37
  167.4 8.9 %fusion.20 = bf16[512,2048]{1,0:T(8,128)(2,1)} fusion(bf16[1,2048,768]{2,1,0:T(8,128)(2,1)} %all-gather.17.cloned.1.call-done, f32[514,768]{1,0:T(8,128)} %multiply_multiply_fusion.2, f32[514,768]{1,0:T(8,128)} %multiply_multiply_fusion.3, f32[768]{0:T(1024)S(1)} %get-tuple-element.12, f32[768]{0:T(1024)S(1)} %get-tuple-element.13, ...), kind=kOutput, calls=%fused_computation.26 | convolution fusion | flops 1617952768 | bytes 14698496 | tf_op jit(solution)/shard_map/dot_general | solution.py:97
  176.4 35.1 %reduce-scatter.3.cloned.1.call-done = bf16[64,2048]{1,0:T(8,128)(2,1)} async-done(((bf16[512,2048]{1,0:T(8,128)(2,1)}), bf16[64,2048]{1,0:T(8,128)(2,1)}) %reduce-scatter.3.cloned.1.call-update) | async-done | bytes 262160 | tf_op jit(solution)/shard_map/reduce_scatter | solution.py:48
  212.3 13.3 %all-gather.3 = bf16[1,256,768]{2,1,0:T(8,128)(2,1)} all-gather(bf16[1,64,768]{2,1,0:T(8,128)(2,1)S(1)} %get-tuple-element.25), channel_id=5, replica_groups=mesh['ra_0'=8,'ra_1'=4,'cb'=8] {'ra_1'}, dimensions={1}, use_global_device_ids=true | all-gather | bytes 491520 | tf_op jit(solution)/shard_map/all_gather | solution.py:37
  225.7 14.2 %all-gather.19.cloned.1.call-done = bf16[512,2048]{1,0:T(8,128)(2,1)} async-done(((bf16[64,2048]{1,0:T(8,128)(2,1)}), bf16[512,2048]{1,0:T(8,128)(2,1)}) %all-gather.19.cloned.1.call-update) | async-done | bytes 2097168 | tf_op jit(solution)/shard_map/all_gather | solution.py:51
  242.4 3.6 collective-permute-start.1
  248.8 80.9 %all-gather.15.cloned.1.call-done = bf16[2048,1536]{1,0:T(8,128)(2,1)} async-done(((bf16[64,1536]{1,0:T(8,128)(2,1)}), bf16[2048,1536]{1,0:T(8,128)(2,1)}) %all-gather.15.cloned.1.call-update) | async-done | bytes 6291472 | tf_op jit(solution)/shard_map/all_gather | solution.py:31
  329.7 5.8 %multiply_multiply_fusion.1 = f32[514,768]{1,0:T(8,128)} fusion(bf16[2048,1536]{1,0:T(8,128)(2,1)} %all-gather.15.cloned.1.call-done, f32[2048]{0:T(1024)S(1)} %bitcast.104, f32[768]{0:T(1024)S(1)} %get-tuple-element.17, f32[514]{0:T(1024)S(1)} %add_rsqrt_fusion, bf16[512,2048]{1,0:T(8,128)(2,1)} %copy-done, bf16[2,2048]{1,0:T(2,128)(2,1)S(1)} %collective-permute-done.1), kind=kOutput, calls=%fused_computation.32 | convolution fusion | flops 1624009728 | bytes 6843400 | tf_op jit(solution)/shard_map/dot_general | solution.py:91
  335.5 3.1 multiply_multiply_fusion
  338.6 36.0 %all-gather.21.cloned.1.call-done = bf16[1,2048,768]{2,1,0:T(8,128)(2,1)} async-done(((bf16[1,256,768]{2,1,0:T(8,128)(2,1)}), bf16[1,2048,768]{2,1,0:T(8,128)(2,1)}) %all-gather.21.cloned.1.call-update) | async-done | bytes 3145744 | tf_op jit(solution)/shard_map/all_gather | solution.py:37
  374.6 8.9 %fusion.23 = bf16[512,2048]{1,0:T(8,128)(2,1)} fusion(bf16[1,2048,768]{2,1,0:T(8,128)(2,1)} %all-gather.21.cloned.1.call-done, f32[514,768]{1,0:T(8,128)} %multiply_multiply_fusion, f32[514,768]{1,0:T(8,128)} %multiply_multiply_fusion.1, f32[768]{0:T(1024)S(1)} %get-tuple-element.15, f32[768]{0:T(1024)S(1)} %get-tuple-element.16, ...), kind=kOutput, calls=%fused_computation.27 | convolution fusion | flops 1617952768 | bytes 14698496 | tf_op jit(solution)/shard_map/dot_general | solution.py:97
  383.5 35.1 %reduce-scatter.5.cloned.1.call-done = bf16[64,2048]{1,0:T(8,128)(2,1)} async-done(((bf16[512,2048]{1,0:T(8,128)(2,1)}), bf16[64,2048]{1,0:T(8,128)(2,1)}) %reduce-scatter.5.cloned.1.call-update) | async-done | bytes 262160 | tf_op jit(solution)/shard_map/reduce_scatter | solution.py:48
  418.6 28.6 %all-gather.23.cloned.1.call-done = bf16[512,2048]{1,0:T(8,128)(2,1)} async-done(((bf16[64,2048]{1,0:T(8,128)(2,1)}), bf16[512,2048]{1,0:T(8,128)(2,1)}) %all-gather.23.cloned.1.call-update) | async-done | bytes 2097168 | tf_op jit(solution)/shard_map/all_gather | solution.py:51
  447.2 3.8 fusion.26
  451.0 2.9 copy.16
  453.9 60.9 %all_to_all.24 = bf16[32,64,512]{2,1,0:T(8,128)(2,1)S(1)} all-to-all(bf16[32,64,512]{2,1,0:T(8,128)(2,1)S(1)} %bitcast.100), channel_id=1, replica_groups=mesh['ra_0'=8,'ra_1'=4,'cb'=8] {'ra_0','ra_1'}, dimensions={0} | all-to-all | bytes 4194304 | tf_op jit(solution)/shard_map/all_to_all | solution.py:107
  (96 shorter events, 35.1 us)
Async XLA Ops:
  6.5 3.0 copy-start.3
  6.5 115.2 %all-gather.13.cloned.1.call-start = ((), (), s32[]{:S(2)}) async-start(), calls=%async_computation.4 | async-start | bytes 6488064 | tf_op jit(solution)/shard_map/all_gather | solution.py:31
  29.8 11.9 %copy-start.4 = (f32[2,64,768]{2,1,0:T(8,128)S(1)}, f32[2,64,768]{2,1,0:T(8,128)}, u32[]{:S(2)}) copy-start(f32[2,64,768]{2,1,0:T(8,128)} %param.18) | copy-start | bytes 1179652
  29.8 26.6 %copy-start.9 = (f32[2,768]{1,0:T(2,128)S(1)}, f32[2,768]{1,0:T(2,128)}, u32[]{:S(2)}) copy-start(f32[2,768]{1,0:T(2,128)} %param.15) | copy-start | bytes 18436
  29.8 26.7 %copy-start.5 = (f32[2,3,768]{2,0,1:T(2,128)S(1)}, f32[2,3,768]{2,0,1:T(2,128)}, u32[]{:S(2)}) copy-start(f32[2,3,768]{2,0,1:T(2,128)} %param.16) | copy-start | bytes 55300
  29.8 26.7 %copy-start.6 = (f32[2,3,768]{2,0,1:T(2,128)S(1)}, f32[2,3,768]{2,0,1:T(2,128)}, u32[]{:S(2)}) copy-start(f32[2,3,768]{2,0,1:T(2,128)} %param.17) | copy-start | bytes 55300
  29.8 26.8 %copy-start.7 = (f32[2,2048]{1,0:T(2,128)S(1)}, f32[2,2048]{1,0:T(2,128)}, u32[]{:S(2)}) copy-start(f32[2,2048]{1,0:T(2,128)} %param.11) | copy-start | bytes 49156
  29.8 74.9 %all-to-all-start = ((bf16[32,64,512]{2,1,0:T(8,128)(2,1)}), bf16[32,64,512]{2,1,0:T(8,128)(2,1)S(1)}, u32[]{:S(2)}, u32[]{:S(2)}) async-start(bf16[32,64,512]{2,1,0:T(8,128)(2,1)} %constant_dynamic-update-slice_fusion), calls=%async_computation | async-start | bytes 4194304 | tf_op jit(solution)/shard_map/all_to_all | solution.py:15
  41.7 125.7 %all-gather.17.cloned.1.call-start = ((), (), s32[]{:S(2)}) async-start(), calls=%async_computation.8 | async-start | bytes 3538944 | tf_op jit(solution)/shard_map/all_gather | solution.py:37
  56.4 155.1 %reduce-scatter.3.cloned.1.call-start = ((), (), s32[]{:S(2)}) async-start(), calls=%async_computation.5 | async-start | bytes 2359296 | tf_op jit(solution)/shard_map/reduce_scatter | solution.py:48
  104.8 1.3 copy-start.2
  106.1 6.9 %copy-start.10 = (f32[2,768]{1,0:T(2,128)S(1)}, f32[2,768]{1,0:T(2,128)}, u32[]{:S(2)}) copy-start(f32[2,768]{1,0:T(2,128)} %param.14) | copy-start | bytes 18436
  109.1 5.5 %collective-permute-start = (bf16[2,2048]{1,0:T(2,128)(2,1)S(1)}, bf16[2,2048]{1,0:T(2,128)(2,1)S(1)}, u32[]{:S(2)}, u32[]{:S(2)}) collective-permute-start(bf16[2,2048]{1,0:T(2,128)(2,1)S(1)} %slice.194), channel_id=1, source_target_pairs={{0,8},{8,16},{16,24},{24,32},{32,40},{40,48},{48,56},{56,64},{64,7... | collective-permute-start | bytes 24584 | tf_op jit(solution)/shard_map/ppermute | solution.py:22
  121.7 5.2 copy-start.11
  176.3 49.4 %copy-start.8 = (f32[2,2048]{1,0:T(2,128)S(1)}, f32[2,2048]{1,0:T(2,128)}, u32[]{:S(2)}) copy-start(f32[2,2048]{1,0:T(2,128)} %param.19) | copy-start | bytes 49156
  176.4 63.6 %all-gather.19.cloned.1.call-start = ((), (), s32[]{:S(2)}) async-start(), calls=%async_computation.9 | async-start | bytes 2359296 | tf_op jit(solution)/shard_map/all_gather | solution.py:51
  211.5 118.2 %all-gather.15.cloned.1.call-start = ((), (), s32[]{:S(2)}) async-start(), calls=%async_computation.6 | async-start | bytes 6488064 | tf_op jit(solution)/shard_map/all_gather | solution.py:31
  212.3 162.3 %all-gather.21.cloned.1.call-start = ((), (), s32[]{:S(2)}) async-start(), calls=%async_computation.10 | async-start | bytes 3538944 | tf_op jit(solution)/shard_map/all_gather | solution.py:37
  225.6 193.0 %reduce-scatter.5.cloned.1.call-start = ((), (), s32[]{:S(2)}) async-start(), calls=%async_computation.7 | async-start | bytes 2359296 | tf_op jit(solution)/shard_map/reduce_scatter | solution.py:48
  242.4 5.6 %copy-start = (bf16[512,2048]{1,0:T(8,128)(2,1)}, bf16[512,2048]{1,0:T(8,128)(2,1)S(1)}, u32[]{:S(2)}) copy-start(bf16[512,2048]{1,0:T(8,128)(2,1)S(1)} %fusion.7) | copy-start | bytes 6291460
  242.4 5.5 %collective-permute-start.1 = (bf16[2,2048]{1,0:T(2,128)(2,1)S(1)}, bf16[2,2048]{1,0:T(2,128)(2,1)S(1)}, u32[]{:S(2)}, u32[]{:S(2)}) collective-permute-start(bf16[2,2048]{1,0:T(2,128)(2,1)S(1)} %slice.204), channel_id=1, source_target_pairs={{0,8},{8,16},{16,24},{24,32},{32,40},{40,48},{48,56},{56,64},{64,7... | collective-permute-start | bytes 24584 | tf_op jit(solution)/shard_map/ppermute | solution.py:22
  329.7 5.8 %copy-start.1 = (bf16[512,2048]{1,0:T(8,128)(2,1)S(1)}, bf16[512,2048]{1,0:T(8,128)(2,1)}, u32[]{:S(2)}) copy-start(bf16[512,2048]{1,0:T(8,128)(2,1)} %copy-done) | copy-start | bytes 6291460
  329.7 5.8 %copy-start.12 = (bf16[2048,1536]{1,0:T(8,128)(2,1)S(1)}, bf16[2048,1536]{1,0:T(8,128)(2,1)}, u32[]{:S(2)}) copy-start(bf16[2048,1536]{1,0:T(8,128)(2,1)} %all-gather.15.cloned.1.call-done) | copy-start | bytes 18874372
  383.5 63.7 %all-gather.23.cloned.1.call-start = ((), (), s32[]{:S(2)}) async-start(), calls=%async_computation.11 | async-start | bytes 2359296 | tf_op jit(solution)/shard_map/all_gather | solution.py:51
Sparse Core Ops, SparseCore 0:
  9.9 111.7 all-gather.12
  123.5 43.8 all-gather.16
  176.5 34.9 reduce-scatter.2
  213.2 26.6 all-gather.18
  242.3 87.3 all-gather.14
  331.4 43.1 all-gather.20
  383.6 34.9 reduce-scatter.4
  420.5 26.6 all-gather.22
